TPU v7x, 256 devices: a whole 4x4x8 slice. The times are simulated.
256 devices in a mesh: sp: 16 (over y, x), tp: 16 (over z, core).
Axes of the slice: x: 4, y: 4, z: 8, core: 2. Of those that a mesh axis runs over, the one named last changes fastest.
Arguments:
- queries: bfloat16 [8192, 2048], P('sp', 'tp'), may hold values from -16 to 16
- key_vectors: bfloat16 [8192, 2048], P('sp', 'tp'), may hold values from -4 to 4
- value_vectors: bfloat16 [8192, 2048], P('sp', 'tp'), may hold values from -5 to 5
- forget_totals: float32 [8192, 16], P('sp', 'tp'), may hold values from -1368 to 0, as said below
- head_gain: float32 [2048], P('tp'), may hold values from 0.1 to 1.9
- stream: bfloat16 [8192, 2048], P(('sp', 'tp')), may hold values from -6 to 6
- out_weight: bfloat16 [2048, 2048], replicated, may hold values from -0.125 to 0.125
- norm_gain: float32 [2048], replicated, may hold values from 0.1 to 1.9
- routing: int32 [8192, 2], P(('sp', 'tp')), may hold values from 0 to 15, all different within a row; in each aligned block of 32 rows (0 to 31, 32 to 63, ...) at most 8 rows name the same one
- route_weights: float32 [8192, 2], P(('sp', 'tp')), may hold values from 0.2 to 1
- gate_weight: bfloat16 [16, 2048, 4096], P('sp', None, 'tp'), may hold values from -0.125 to 0.125
- up_weight: bfloat16 [16, 2048, 4096], P('sp', None, 'tp'), may hold values from -0.125 to 0.125
- down_weight: bfloat16 [16, 4096, 2048], P('sp', 'tp'), may hold values from -0.09375 to 0.09375
Outputs:
- layer_out: bfloat16 [8192, 2048], P(('sp', 'tp'))
Inputs may be any that keep to these rules, and one draw needn't show every extreme that they name: `forget_totals`: along the positions, the values of each head never rise. `routing`: A token's 2 experts differ. Within the tokens of one device (aligned blocks of 32 rows) no expert is named more than 8 times.
All inputs are finite; a program needn't handle non-finite values.
Results may differ from a plain program's by a relative error of at most 0.01145.
Values may be sent and summed in bfloat16 or wider, within the bound.
A program may use at most 128 MiB of HBM per device.

v0:
```python
from functools import partial
import jax
import jax.numpy as jnp
from jax import lax
from jax.sharding import PartitionSpec as P

HD = 128
TOP = 2
masked_score = -1e30


def sent_together(arrays, axis, dim, along):
    ends, at = ([], 0)
    for a in arrays[:-1]:
        at += a.shape[along]
        ends.append(at)
    both = jnp.concatenate(arrays, axis=along)
    return tuple(jnp.split(lax.all_gather(both, axis, axis=dim, tiled=True), ends, axis=along))


def attend_block(
    totals, query_rows, query_gate, query_pos, key_rows, value_rows, key_gate, key_pos
):
    run_max, run_sum, run_acc = totals
    scores = jnp.einsum("qhd,khd->hqk", query_rows, key_rows, preferred_element_type=jnp.float32)
    scores = scores * HD ** (-0.5) + query_gate[:, :, None] - key_gate[:, None, :]
    visible = (key_pos[None, :] <= query_pos[:, None])[None]
    scores = jnp.where(visible, scores, masked_score)
    new_max = jnp.maximum(run_max, jnp.max(scores, axis=2))
    lifted = jnp.where(visible, jnp.exp(scores - new_max[:, :, None]), 0.0)
    rescale = jnp.exp(run_max - new_max)
    new_sum = run_sum * rescale + jnp.sum(lifted, axis=2)
    product = jnp.einsum(
        "hqk,khd->hqd", lifted.astype(jnp.bfloat16), value_rows, preferred_element_type=jnp.float32
    )
    new_acc = run_acc * rescale[:, :, None] + product
    return (new_max, new_sum, new_acc)


def keep_totals(totals_in):
    return totals_in


def make_folder(segments, gathered_gates):

    def fold_keys(state_all, key_piece, first_key):
        key_part, value_part = key_piece
        key_total = key_part.shape[0]
        block_len = min(512, key_total)
        heads_dev = segments[0][0].shape[1]
        key_part = key_part.reshape(key_total, heads_dev, HD)
        value_part = value_part.reshape(key_total, heads_dev, HD)

        def one_block(block_index, state_now):
            offset = block_index * block_len
            key_rows = lax.dynamic_slice_in_dim(key_part, offset, block_len, 0)
            value_rows = lax.dynamic_slice_in_dim(value_part, offset, block_len, 0)
            key_pos = offset + jnp.arange(block_len, dtype=jnp.int32)
            key_gate = jnp.transpose(lax.dynamic_slice_in_dim(gathered_gates, offset, block_len, 0))
            updated = []
            for segment, totals_in in zip(segments, state_now):
                query_rows, query_gate, query_pos = segment
                needed = offset <= query_pos[-1]
                advance = partial(
                    attend_block,
                    query_rows=query_rows,
                    query_gate=query_gate,
                    query_pos=query_pos,
                    key_rows=key_rows,
                    value_rows=value_rows,
                    key_gate=key_gate,
                    key_pos=key_pos,
                )
                updated.append(lax.cond(needed, advance, keep_totals, totals_in))
            return tuple(updated)

        return lax.fori_loop(0, key_total // block_len, one_block, state_all)

    return fold_keys


def on_device(
    queries,
    key_vectors,
    value_vectors,
    forget_totals,
    head_gain,
    stream,
    out_weight,
    norm_gain,
    routing,
    route_weights,
    gate_weight,
    up_weight,
    down_weight,
):
    tok_count = queries.shape[0]
    heads_dev = queries.shape[1] // HD
    sp_index = lax.axis_index("sp")
    sp_count = lax.axis_size("sp")
    gathered_gates = lax.all_gather(forget_totals, "sp", axis=0, tiled=True)
    first_pos = sp_index * tok_count
    query_pos = first_pos + jnp.arange(tok_count, dtype=jnp.int32)
    query_gate = jnp.transpose(lax.dynamic_slice_in_dim(gathered_gates, first_pos, tok_count, 0))
    segments = [(queries.reshape(tok_count, heads_dev, HD), query_gate, query_pos)]
    starting = (
        (
            jnp.full((heads_dev, tok_count), masked_score, jnp.float32),
            jnp.zeros((heads_dev, tok_count), jnp.float32),
            jnp.zeros((heads_dev, tok_count, HD), jnp.float32),
        ),
    )
    folder = make_folder(segments, gathered_gates)
    totals = folder(starting, sent_together((key_vectors, value_vectors), "sp", 0, 1), jnp.int32(0))
    run_max, run_sum, run_acc = totals[0]
    attended = run_acc / run_sum[:, :, None]
    inverse_rms = lax.rsqrt(jnp.mean(attended * attended, axis=2, keepdims=True) + 1e-06)
    normed = attended * inverse_rms * head_gain.reshape(heads_dev, 1, HD)
    head_out = (
        jnp.transpose(normed, (1, 0, 2)).reshape(tok_count, heads_dev * HD).astype(jnp.bfloat16)
    )
    token_heads = lax.all_to_all(head_out, "tp", split_axis=0, concat_axis=1, tiled=True)
    mixed_rows = jnp.dot(token_heads, out_weight, preferred_element_type=jnp.float32)
    resid_sum = stream.astype(jnp.float32) + mixed_rows
    center = resid_sum - jnp.mean(resid_sum, axis=1, keepdims=True)
    normed_rows = (
        center * lax.rsqrt(jnp.mean(center * center, axis=1, keepdims=True) + 1e-05) * norm_gain
    ).astype(jnp.bfloat16)
    row_count = normed_rows.shape[0]
    capacity = max(2, 2 * TOP * row_count // sp_count)
    flat_expert = routing.reshape(-1)
    onehot = (flat_expert[:, None] == jnp.arange(sp_count, dtype=jnp.int32)[None, :]).astype(
        jnp.int32
    )
    earlier = jnp.cumsum(onehot, axis=0) - onehot
    slot_index = flat_expert * capacity + jnp.sum(earlier * onehot, axis=1)
    slot_grid = slot_index.reshape(row_count, TOP)
    slot_ids = jnp.arange(sp_count * capacity, dtype=jnp.int32)
    placing = jnp.sum(
        (slot_grid[None, :, :] == slot_ids[:, None, None]).astype(jnp.float32), axis=2
    ).astype(jnp.bfloat16)
    outgoing = jnp.dot(placing, normed_rows, preferred_element_type=jnp.float32).astype(
        jnp.bfloat16
    )
    outgoing = outgoing.reshape(sp_count, capacity, normed_rows.shape[1])
    arrived = lax.all_to_all(outgoing, "sp", split_axis=0, concat_axis=0, tiled=True)
    row_piece = lax.all_gather(arrived.reshape(-1, arrived.shape[2]), "tp", axis=0, tiled=True)
    gate_pre = jnp.dot(row_piece, gate_weight[0], preferred_element_type=jnp.float32)
    up_pre = jnp.dot(row_piece, up_weight[0], preferred_element_type=jnp.float32)
    hidden = (jax.nn.silu(gate_pre) * up_pre).astype(jnp.bfloat16)
    summed = lax.psum_scatter(
        jnp.dot(hidden, down_weight[0], preferred_element_type=jnp.float32).astype(jnp.bfloat16),
        "tp",
        scatter_dimension=0,
        tiled=True,
    )
    expert_out = summed.reshape(sp_count, capacity, -1)
    returned = lax.all_to_all(expert_out, "sp", split_axis=0, concat_axis=0, tiled=True)
    picked = returned.reshape(sp_count * capacity, -1)[slot_index].astype(jnp.float32)
    weighted = picked * route_weights.reshape(-1)[:, None]
    routed = jnp.sum(weighted.reshape(row_count, TOP, -1), axis=1)
    return (resid_sum + routed).astype(jnp.bfloat16)


def solution(mesh):
    in_specs = (
        P("sp", "tp"),
        P("sp", "tp"),
        P("sp", "tp"),
        P("sp", "tp"),
        P("tp"),
        P(("sp", "tp"), None),
        P(),
        P(),
        P(("sp", "tp"), None),
        P(("sp", "tp"), None),
        P("sp", None, "tp"),
        P("sp", None, "tp"),
        P("sp", "tp", None),
    )
    out_specs = P(("sp", "tp"), None)
    return jax.shard_map(
        on_device, mesh=mesh, in_specs=in_specs, out_specs=out_specs, check_vma=False
    )
```

profile of v0, /device:TPU:2, one launch (start us, length us, event | category | flops | bytes accessed | tf_op | source)
XLA Modules:
  0.0 334.1 jit_solution(2829663943095619503)
XLA Ops:
  6.5 1.8 pad_maximum_fusion
  8.3 0.8 copy.26
  9.7 23.4 %all_gather.10 = f32[8192,1]{0,1:T(1,128)S(1)} all-gather(f32[512,1]{0,1:T(1,128)} %param.20), channel_id=1, replica_groups=mesh['sp'=16,'tp'=16] {'sp'}, dimensions={0}, use_global_device_ids=true | all-gather | bytes 34816 | tf_op jit(solution)/shard_map/all_gather | solution.py:101
  33.1 36.1 %all-gather.3.cloned.1.call-done = bf16[8192,256]{1,0:T(8,128)(2,1)} async-done(((bf16[512,256]{1,0:T(8,128)(2,1)}), bf16[8192,256]{1,0:T(8,128)(2,1)}) %all-gather.3.cloned.1.call-update) | async-done | bytes 4194320 | tf_op jit(solution)/shard_map/all_gather | solution.py:18
  69.2 3.8 %slice_bitcast_fusion = (bf16[8192,1,128]{2,0,1:T(8,128)(2,1)S(1)}, bf16[8192,1,128]{2,0,1:T(8,128)(2,1)}) fusion(bf16[8192,256]{1,0:T(8,128)(2,1)} %all-gather.3.cloned.1.call-done), kind=kLoop, calls=%fused_computation.33 | loop fusion | bytes 8388608 | tf_op jit(solution)/shard_map/reshape | solution.py:52
  73.1 23.5 %while.17 = (s32[]{:T(128)}, f32[1,512]{1,0:T(1,128)S(1)}, f32[1,512]{1,0:T(1,128)S(1)}, f32[1,512,128]{2,1,0:T(8,128)S(1)}, s32[512]{0:T(512)S(1)}, /*index=5*/...) while((s32[]{:T(128)}, f32[1,512]{1,0:T(1,128)S(1)}, ...), condition=%wide.region_5.6_spmd, body=%wide.region_0.5_spmd.sunk | while | flops 138020352 | bytes 4122969 | solution.py:77
  73.1 0.6 slice.10
  74.3 2.2 conditional.2
  74.3 1.4 fusion.38
  75.7 0.2 fusion.6
  76.0 0.5 fusion.4
  76.5 0.6 slice.10
  77.7 2.2 conditional.2
  77.7 1.4 fusion.38
  79.1 0.2 fusion.6
  79.4 0.5 fusion.4
  79.9 0.6 slice.10
  81.1 0.6 slice.10
  82.3 0.6 slice.10
  83.5 0.6 slice.10
  84.7 0.6 slice.10
  85.9 0.6 slice.10
  87.1 0.6 slice.10
  88.3 0.6 slice.10
  89.5 0.6 slice.10
  90.6 0.6 slice.10
  91.8 0.6 slice.10
  93.0 0.6 slice.10
  94.2 0.6 slice.10
  95.4 0.6 slice.10
  96.6 0.2 multiply_reduce_fusion.2
  96.8 0.9 multiply_convert_fusion.1
  97.7 7.1 %all-to-all-start = ((bf16[16,32,128]{2,1,0:T(8,128)(2,1)}), bf16[16,32,128]{2,1,0:T(8,128)(2,1)S(1)}, u32[]{:S(2)}, u32[]{:S(2)}) async-start(bf16[16,32,128]{2,1,0:T(8,128)(2,1)} %bitcast.16), calls=%async_computation | async-start | bytes 262144 | tf_op jit(solution)/shard_map/all_to_all | solution.py:122
  105.1 8.4 %all-to-all-done = bf16[16,32,128]{2,1,0:T(8,128)(2,1)S(1)} async-done(((bf16[16,32,128]{2,1,0:T(8,128)(2,1)}), bf16[16,32,128]{2,1,0:T(8,128)(2,1)S(1)}, u32[]{:S(2)}, u32[]{:S(2)}) %all-to-all-start) | async-done | bytes 131104 | tf_op jit(solution)/shard_map/all_to_all | solution.py:122
  113.5 5.0 %fusion.39 = (f32[32]{0:T(128)S(1)}, f32[32,2048]{1,0:T(8,128)S(1)}) fusion(bf16[2048,2048]{1,0:T(8,128)(2,1)} %param.23, bf16[32,2048]{1,0:T(8,128)(2,1)} %param.22, bf16[16,32,128]{2,1,0:T(8,128)(2,1)S(1)} %all-to-all-done), kind=kOutput, calls=%fused_computation.72 | convolution fusion | flops 268632032 | bytes 8913024 | tf_op jit(solution)/shard_map/dot_general | solution.py:123
  118.5 0.2 multiply_reduce_fusion.1
  118.8 0.3 fusion.21
  119.1 46.6 %all_to_all.26 = bf16[16,8,2048]{2,1,0:T(8,128)(2,1)} all-to-all(bf16[16,8,2048]{2,1,0:T(8,128)(2,1)S(1)} %fusion.21), channel_id=1, replica_groups=mesh['sp'=16,'tp'=16] {'sp'}, dimensions={0} | all-to-all | bytes 1048576 | tf_op jit(solution)/shard_map/all_to_all | solution.py:146
  165.8 49.9 %all-gather.5.cloned.1.call-done = bf16[2048,2048]{1,0:T(8,128)(2,1)} async-done(((bf16[128,2048]{1,0:T(8,128)(2,1)}), bf16[2048,2048]{1,0:T(8,128)(2,1)}) %all-gather.5.cloned.1.call-update) | async-done | bytes 8388624 | tf_op jit(solution)/shard_map/all_gather | solution.py:147
  215.8 7.1 %fusion.25 = f32[2048,256]{1,0:T(8,128)} fusion(bf16[2048,2048]{1,0:T(8,128)(2,1)} %all-gather.5.cloned.1.call-done, bf16[1,2048,256]{2,1,0:T(8,128)(2,1)S(1)} %copy-done.4), kind=kOutput, calls=%fused_computation.37 | convolution fusion | flops 2147483648 | bytes 11534336 | tf_op jit(solution)/shard_map/dot_general | solution.py:148
  222.9 16.8 %convolution_convert_fusion = bf16[2048,2048]{1,0:T(8,128)(2,1)} fusion(bf16[2048,2048]{1,0:T(8,128)(2,1)} %all-gather.5.cloned.1.call-done, f32[2048,256]{1,0:T(8,128)} %fusion.25, bf16[1,256,2048]{2,1,0:T(8,128)(2,1)S(1)} %copy-done, bf16[1,2048,256]{2,1,0:T(8,128)(2,1)} %param.28), kind=kOutput, calls=%fused_computation.27 | convolution fusion | flops 4302307328 | bytes 20971520 | tf_op jit(solution)/shard_map/dot_general | solution.py:152
  239.7 69.3 %reduce-scatter.2.cloned.1.call-done = bf16[128,2048]{1,0:T(8,128)(2,1)} async-done(((bf16[2048,2048]{1,0:T(8,128)(2,1)}), bf16[128,2048]{1,0:T(8,128)(2,1)}) %reduce-scatter.2.cloned.1.call-update) | async-done | bytes 524304 | tf_op jit(solution)/shard_map/reduce_scatter | solution.py:151
  309.0 7.3 %all-to-all-start.2 = ((bf16[16,8,2048]{2,1,0:T(8,128)(2,1)}), bf16[16,8,2048]{2,1,0:T(8,128)(2,1)S(1)}, u32[]{:S(2)}, u32[]{:S(2)}) async-start(bf16[16,8,2048]{2,1,0:T(8,128)(2,1)} %bitcast.76), calls=%async_computation.3 | async-start | bytes 1048576 | tf_op jit(solution)/shard_map/all_to_all | solution.py:158
  316.5 8.6 %all-to-all-done.2 = bf16[16,8,2048]{2,1,0:T(8,128)(2,1)S(1)} async-done(((bf16[16,8,2048]{2,1,0:T(8,128)(2,1)}), bf16[16,8,2048]{2,1,0:T(8,128)(2,1)S(1)}, u32[]{:S(2)}, u32[]{:S(2)}) %all-to-all-start.2) | async-done | bytes 524320 | tf_op jit(solution)/shard_map/all_to_all | solution.py:158
  325.1 0.7 gather_fusion
  325.9 0.3 reshape.179
  326.2 0.7 multiply_reduce_fusion
  326.9 0.7 add_convert_fusion
  (76 shorter events, 1.5 us)
Async XLA Ops:
  6.5 216.3 %copy-start = (bf16[1,256,2048]{2,1,0:T(8,128)(2,1)S(1)}, bf16[1,256,2048]{2,1,0:T(8,128)(2,1)}, u32[]{:S(2)}) copy-start(bf16[1,256,2048]{2,1,0:T(8,128)(2,1)} %param.29) | copy-start | bytes 3145732
  6.5 62.7 %all-gather.3.cloned.1.call-start = ((), (), s32[]{:S(2)}) async-start(), calls=%async_computation.4 | async-start | bytes 4456448 | tf_op jit(solution)/shard_map/all_gather | solution.py:18
  73.1 23.8 %copy-start.3 = (f32[128]{0:T(128)S(1)}, f32[128]{0:T(128)}, u32[]{:S(2)}) copy-start(f32[128]{0:T(128)} %param.21) | copy-start | bytes 1540
  97.7 15.8 %all-to-all-start = ((bf16[16,32,128]{2,1,0:T(8,128)(2,1)}), bf16[16,32,128]{2,1,0:T(8,128)(2,1)S(1)}, u32[]{:S(2)}, u32[]{:S(2)}) async-start(bf16[16,32,128]{2,1,0:T(8,128)(2,1)} %bitcast.16), calls=%async_computation | async-start | bytes 262144 | tf_op jit(solution)/shard_map/all_to_all | solution.py:122
  104.8 110.9 %all-gather.5.cloned.1.call-start = ((), (), s32[]{:S(2)}) async-start(), calls=%async_computation.5 | async-start | bytes 8912896 | tf_op jit(solution)/shard_map/all_gather | solution.py:147
  105.1 13.7 %copy-start.1 = (f32[2048]{0:T(1024)S(1)}, f32[2048]{0:T(1024)}, u32[]{:S(2)}) copy-start(f32[2048]{0:T(1024)} %param.24) | copy-start | bytes 24580
  118.5 97.3 %copy-start.4 = (bf16[1,2048,256]{2,1,0:T(8,128)(2,1)S(1)}, bf16[1,2048,256]{2,1,0:T(8,128)(2,1)}, u32[]{:S(2)}) copy-start(bf16[1,2048,256]{2,1,0:T(8,128)(2,1)} %param.27) | copy-start | bytes 3145732
  165.8 143.2 %reduce-scatter.2.cloned.1.call-start = ((), (), s32[]{:S(2)}) async-start(), calls=%async_computation.6 | async-start | bytes 8912896 | tf_op jit(solution)/shard_map/reduce_scatter | solution.py:151
  239.7 76.8 %copy-start.2 = (f32[32,2]{0,1:T(2,128)S(1)}, f32[32,2]{0,1:T(2,128)}, u32[]{:S(2)}) copy-start(f32[32,2]{0,1:T(2,128)} %param.26) | copy-start | bytes 772
  309.0 16.1 %all-to-all-start.2 = ((bf16[16,8,2048]{2,1,0:T(8,128)(2,1)}), bf16[16,8,2048]{2,1,0:T(8,128)(2,1)S(1)}, u32[]{:S(2)}, u32[]{:S(2)}) async-start(bf16[16,8,2048]{2,1,0:T(8,128)(2,1)} %bitcast.76), calls=%async_computation.3 | async-start | bytes 1048576 | tf_op jit(solution)/shard_map/all_to_all | solution.py:158
Sparse Core Ops, SparseCore 0:
  9.8 59.4 all-gather.2
  165.9 49.8 all-gather.4
  239.8 69.1 reduce-scatter.1
where the time goes:
time: 335 us; the launch traced here: 334 us
  waiting for transfers between devices  172 us (51%)
  blocking collectives  70.1 us (21%)
  matrix products  33 us (10%)
  local copies, waits for them, and re-layouts  15.5 us (5%)
  starting transfers between devices  14.5 us (4%)
  between operations  13.3 us (4%)
  loops' own time  9.92 us (3%)
  other arithmetic  5.49 us (2%)
    reduce_scatter x1, waiting for transfers between devices, on_device(): lax.psum_scatter(jnp.dot(hidden, down_weight[0], preferred_element_type=j...  69.3 us
    all_gather x1, waiting for transfers between devices, on_device(): lax.all_gather(arrived.reshape(-1, arrived.shape[2]), 'tp', axis=0, tiled...  49.9 us
    all_to_all x1, blocking collectives, on_device(): lax.all_to_all(outgoing, 'sp', split_axis=0, concat_axis=0, tiled=True)  46.6 us
    all_gather x1, waiting for transfers between devices, sent_together(): lax.all_gather(both, axis, axis=dim, tiled=True)  36.1 us
    all_gather x1, blocking collectives, on_device(): gathered_gates = lax.all_gather(forget_totals, 'sp', axis=0, tiled=True)  23.4 us
    dot_general x1, matrix products, on_device(): jnp.dot(hidden, down_weight[0], preferred_element_type=jnp.float32)  16.8 us
    another operation x1, loops' own time, fold_keys(): return lax.fori_loop(0, key_total // block_len, one_block, state_all)  9.6 us
    slice x16, local copies, waits for them, and re-layouts, one_block(): needed = offset <= query_pos[-1]  9.2 us
  transfers between devices with their start and end apart: 5, of which 5 were waited for; matrix products, arithmetic and copies ran while one was open for 1% of the time, Pallas kernels for 0%

commit v1 on v0

--- a/solution.py
+++ b/solution.py
@@ -144,7 +144,10 @@
     )
     outgoing = outgoing.reshape(sp_count, capacity, normed_rows.shape[1])
     arrived = lax.all_to_all(outgoing, "sp", split_axis=0, concat_axis=0, tiled=True)
-    row_piece = lax.all_gather(arrived.reshape(-1, arrived.shape[2]), "tp", axis=0, tiled=True)
+    z_in = arrived.reshape(-1, arrived.shape[2])
+    row_piece = jnp.concatenate(
+        lax.all_to_all(jnp.stack(lax.axis_size("tp") * [z_in], axis=0), "tp", 0, 0), 0
+    )
     gate_pre = jnp.dot(row_piece, gate_weight[0], preferred_element_type=jnp.float32)
     up_pre = jnp.dot(row_piece, up_weight[0], preferred_element_type=jnp.float32)
     hidden = (jax.nn.silu(gate_pre) * up_pre).astype(jnp.bfloat16)

time: 335 us -> 471 us (1.41)
  blocking collectives: 70.1 us -> 257 us
  waiting for transfers between devices: 172 us -> 120 us
    all_to_all x0 -> x1, blocking collectives: none -> 187 us  [on_device(): lax.all_to_all(jnp.stack(lax.axis_size('tp') * [z_in], axis=0), 'tp', 0, 0)]
    all_gather x1 -> x0, waiting for transfers between devices: 49.9 us -> none  [on_device(): lax.all_gather(arrived.reshape(-1, arrived.shape[2]), 'tp', axis=0, tiled...]
  transfers between devices with their start and end apart: 5 -> 4, of which waited for: 5 -> 4; matrix products, arithmetic and copies ran while one was open for 1% -> 0% of each run, Pallas kernels for 0% -> 0%
where the time goes in v1:
time: 471 us; the launch traced here: 470 us
  blocking collectives  257 us (55%)
  waiting for transfers between devices  120 us (25%)
  matrix products  29.8 us (6%)
  local copies, waits for them, and re-layouts  19.7 us (4%)
  starting transfers between devices  14.5 us (3%)
  between operations  13.6 us (3%)
  loops' own time  9.92 us (2%)
  other arithmetic  5.5 us (1%)
    all_to_all x1, blocking collectives, on_device(): lax.all_to_all(jnp.stack(lax.axis_size('tp') * [z_in], axis=0), 'tp', 0, 0)  187 us
    reduce_scatter x1, waiting for transfers between devices, on_device(): lax.psum_scatter(jnp.dot(hidden, down_weight[0], preferred_element_type=j...  66.7 us
    all_to_all x1, blocking collectives, on_device(): lax.all_to_all(outgoing, 'sp', split_axis=0, concat_axis=0, tiled=True)  46.6 us
    all_gather x1, waiting for transfers between devices, sent_together(): lax.all_gather(both, axis, axis=dim, tiled=True)  36.1 us
    all_gather x1, blocking collectives, on_device(): gathered_gates = lax.all_gather(forget_totals, 'sp', axis=0, tiled=True)  23.4 us
    dot_general x1, matrix products, on_device(): jnp.dot(hidden, down_weight[0], preferred_element_type=jnp.float32)  16.8 us
    another operation x1, loops' own time, fold_keys(): return lax.fori_loop(0, key_total // block_len, one_block, state_all)  9.6 us
  transfers between devices with their start and end apart: 4, of which 4 were waited for; matrix products, arithmetic and copies ran while one was open for 0% of the time, Pallas kernels for 0%

profile of v1, /device:TPU:2, one launch (start us, length us, event | category | flops | bytes accessed | tf_op | source)
XLA Modules:
  0.0 469.9 jit_solution(1481307971937641133)
XLA Ops:
  6.5 1.8 pad_maximum_fusion
  8.3 0.8 copy.26
  9.7 23.4 %all_gather.7 = f32[8192,1]{0,1:T(1,128)S(1)} all-gather(f32[512,1]{0,1:T(1,128)} %param.20), channel_id=1, replica_groups=mesh['sp'=16,'tp'=16] {'sp'}, dimensions={0}, use_global_device_ids=true | all-gather | bytes 34816 | tf_op jit(solution)/shard_map/all_gather | solution.py:101
  33.1 36.1 %all-gather.2.cloned.1.call-done = bf16[8192,256]{1,0:T(8,128)(2,1)} async-done(((bf16[512,256]{1,0:T(8,128)(2,1)}), bf16[8192,256]{1,0:T(8,128)(2,1)}) %all-gather.2.cloned.1.call-update) | async-done | bytes 4194320 | tf_op jit(solution)/shard_map/all_gather | solution.py:18
  69.2 3.8 slice_bitcast_fusion
  73.1 23.5 %while.17 = (s32[]{:T(128)}, f32[1,512]{1,0:T(1,128)S(1)}, f32[1,512]{1,0:T(1,128)S(1)}, f32[1,512,128]{2,1,0:T(8,128)S(1)}, s32[512]{0:T(512)S(1)}, /*index=5*/...) while((s32[]{:T(128)}, f32[1,512]{1,0:T(1,128)S(1)}, ...), condition=%wide.region_5.6_spmd, body=%wide.region_0.5_spmd.sunk | while | flops 138020352 | bytes 4122969 | solution.py:77
  73.1 0.6 slice.10
  74.3 2.2 conditional.2
  74.3 1.4 fusion.38
  75.7 0.2 fusion.6
  76.0 0.5 fusion.4
  76.5 0.6 slice.10
  77.7 2.2 conditional.2
  77.7 1.4 fusion.38
  79.1 0.2 fusion.6
  79.4 0.5 fusion.4
  79.9 0.6 slice.10
  81.1 0.6 slice.10
  82.3 0.6 slice.10
  83.5 0.6 slice.10
  84.7 0.6 slice.10
  85.9 0.6 slice.10
  87.1 0.6 slice.10
  88.3 0.6 slice.10
  89.5 0.6 slice.10
  90.6 0.6 slice.10
  91.8 0.6 slice.10
  93.0 0.6 slice.10
  94.2 0.6 slice.10
  95.4 0.6 slice.10
  96.8 0.9 multiply_convert_fusion.1
  97.7 7.1 %all-to-all-start = ((bf16[16,32,128]{2,1,0:T(8,128)(2,1)}), bf16[16,32,128]{2,1,0:T(8,128)(2,1)S(1)}, u32[]{:S(2)}, u32[]{:S(2)}) async-start(bf16[16,32,128]{2,1,0:T(8,128)(2,1)} %bitcast.16), calls=%async_computation | async-start | bytes 262144 | tf_op jit(solution)/shard_map/all_to_all | solution.py:122
  105.1 8.4 %all-to-all-done = bf16[16,32,128]{2,1,0:T(8,128)(2,1)S(1)} async-done(((bf16[16,32,128]{2,1,0:T(8,128)(2,1)}), bf16[16,32,128]{2,1,0:T(8,128)(2,1)S(1)}, u32[]{:S(2)}, u32[]{:S(2)}) %all-to-all-start) | async-done | bytes 131104 | tf_op jit(solution)/shard_map/all_to_all | solution.py:122
  113.5 5.0 %fusion.39 = (f32[32]{0:T(128)S(1)}, f32[32,2048]{1,0:T(8,128)S(1)}) fusion(bf16[2048,2048]{1,0:T(8,128)(2,1)} %param.23, bf16[32,2048]{1,0:T(8,128)(2,1)} %param.22, bf16[16,32,128]{2,1,0:T(8,128)(2,1)S(1)} %all-to-all-done), kind=kOutput, calls=%fused_computation.72 | convolution fusion | flops 268632032 | bytes 8913024 | tf_op jit(solution)/shard_map/dot_general | solution.py:123
  118.8 0.3 fusion.21
  119.1 46.6 %all_to_all.31 = bf16[16,8,2048]{2,1,0:T(8,128)(2,1)S(1)} all-to-all(bf16[16,8,2048]{2,1,0:T(8,128)(2,1)S(1)} %fusion.21), channel_id=1, replica_groups=mesh['sp'=16,'tp'=16] {'sp'}, dimensions={0} | all-to-all | bytes 1048576 | tf_op jit(solution)/shard_map/all_to_all | solution.py:146
  165.7 1.1 stack.3
  166.7 187.3 %all_to_all.32 = bf16[16,128,2048]{2,1,0:T(8,128)(2,1)S(1)} all-to-all(bf16[16,128,2048]{2,1,0:T(8,128)(2,1)S(1)} %stack.3), channel_id=1, replica_groups=mesh['sp'=16,'tp'=16] {'tp'}, dimensions={0} | all-to-all | bytes 16777216 | tf_op jit(solution)/shard_map/all_to_all | solution.py:149
  354.0 3.2 copy-done.1
  357.2 3.8 fusion.25
  361.0 16.8 %convolution_convert_fusion = bf16[2048,2048]{1,0:T(8,128)(2,1)} fusion(bf16[2048,2048]{1,0:T(8,128)(2,1)} %bitcast.75, f32[2048,256]{1,0:T(8,128)} %fusion.25, bf16[1,256,2048]{2,1,0:T(8,128)(2,1)S(1)} %copy-done, bf16[1,2048,256]{2,1,0:T(8,128)(2,1)} %param.28), kind=kOutput, calls=%fused_computation.27 | convolution fusion | flops 4302307328 | bytes 20971520 | tf_op jit(solution)/shard_map/dot_general | solution.py:155
  377.9 66.7 %reduce-scatter.2.cloned.1.call-done = bf16[128,2048]{1,0:T(8,128)(2,1)} async-done(((bf16[2048,2048]{1,0:T(8,128)(2,1)}), bf16[128,2048]{1,0:T(8,128)(2,1)}) %reduce-scatter.2.cloned.1.call-update) | async-done | bytes 524304 | tf_op jit(solution)/shard_map/reduce_scatter | solution.py:154
  444.5 7.3 %all-to-all-start.3 = ((bf16[16,8,2048]{2,1,0:T(8,128)(2,1)}), bf16[16,8,2048]{2,1,0:T(8,128)(2,1)S(1)}, u32[]{:S(2)}, u32[]{:S(2)}) async-start(bf16[16,8,2048]{2,1,0:T(8,128)(2,1)} %bitcast.79), calls=%async_computation.4 | async-start | bytes 1048576 | tf_op jit(solution)/shard_map/all_to_all | solution.py:161
  452.0 8.6 %all-to-all-done.3 = bf16[16,8,2048]{2,1,0:T(8,128)(2,1)S(1)} async-done(((bf16[16,8,2048]{2,1,0:T(8,128)(2,1)}), bf16[16,8,2048]{2,1,0:T(8,128)(2,1)S(1)}, u32[]{:S(2)}, u32[]{:S(2)}) %all-to-all-start.3) | async-done | bytes 524320 | tf_op jit(solution)/shard_map/all_to_all | solution.py:161
  460.6 0.7 gather_fusion
  461.4 0.3 reshape.181
  461.7 0.7 multiply_reduce_fusion
  462.4 0.7 add_convert_fusion
  (77 shorter events, 1.8 us)
Async XLA Ops:
  6.5 354.5 %copy-start = (bf16[1,256,2048]{2,1,0:T(8,128)(2,1)S(1)}, bf16[1,256,2048]{2,1,0:T(8,128)(2,1)}, u32[]{:S(2)}) copy-start(bf16[1,256,2048]{2,1,0:T(8,128)(2,1)} %param.29) | copy-start | bytes 3145732
  6.5 62.7 %all-gather.2.cloned.1.call-start = ((), (), s32[]{:S(2)}) async-start(), calls=%async_computation.5 | async-start | bytes 4456448 | tf_op jit(solution)/shard_map/all_gather | solution.py:18
  73.1 23.8 %copy-start.4 = (f32[128]{0:T(128)S(1)}, f32[128]{0:T(128)}, u32[]{:S(2)}) copy-start(f32[128]{0:T(128)} %param.21) | copy-start | bytes 1540
  97.7 15.8 %all-to-all-start = ((bf16[16,32,128]{2,1,0:T(8,128)(2,1)}), bf16[16,32,128]{2,1,0:T(8,128)(2,1)S(1)}, u32[]{:S(2)}, u32[]{:S(2)}) async-start(bf16[16,32,128]{2,1,0:T(8,128)(2,1)} %bitcast.16), calls=%async_computation | async-start | bytes 262144 | tf_op jit(solution)/shard_map/all_to_all | solution.py:122
  104.8 339.7 %reduce-scatter.2.cloned.1.call-start = ((), (), s32[]{:S(2)}) async-start(), calls=%async_computation.6 | async-start | bytes 8912896 | tf_op jit(solution)/shard_map/reduce_scatter | solution.py:154
  105.0 13.7 %copy-start.2 = (f32[2048]{0:T(1024)S(1)}, f32[2048]{0:T(1024)}, u32[]{:S(2)}) copy-start(f32[2048]{0:T(1024)} %param.24) | copy-start | bytes 24580
  166.7 190.5 %copy-start.5 = (bf16[1,2048,256]{2,1,0:T(8,128)(2,1)S(1)}, bf16[1,2048,256]{2,1,0:T(8,128)(2,1)}, u32[]{:S(2)}) copy-start(bf16[1,2048,256]{2,1,0:T(8,128)(2,1)} %param.27) | copy-start | bytes 3145732
  354.0 3.2 copy-start.1
  377.9 74.1 %copy-start.3 = (f32[32,2]{0,1:T(2,128)S(1)}, f32[32,2]{0,1:T(2,128)}, u32[]{:S(2)}) copy-start(f32[32,2]{0,1:T(2,128)} %param.26) | copy-start | bytes 772
  444.5 16.1 %all-to-all-start.3 = ((bf16[16,8,2048]{2,1,0:T(8,128)(2,1)}), bf16[16,8,2048]{2,1,0:T(8,128)(2,1)S(1)}, u32[]{:S(2)}, u32[]{:S(2)}) async-start(bf16[16,8,2048]{2,1,0:T(8,128)(2,1)} %bitcast.79), calls=%async_computation.4 | async-start | bytes 1048576 | tf_op jit(solution)/shard_map/all_to_all | solution.py:161
Sparse Core Ops, SparseCore 0:
  9.8 59.4 all-gather.1
  378.0 66.4 reduce-scatter.1
